TPU v7x, 32 devices: a whole 2x2x4 slice. The times are simulated.
32 devices in a mesh: sp: 4 (over z), tp: 4 (over y, x), dp: 2 (over core).
Axes of the slice: x: 2, y: 2, z: 4, core: 2. Of those that a mesh axis runs over, the one named last changes fastest.
Arguments:
- latent_in: bfloat16 [3072, 2048], P(('dp', 'sp', 'tp')), parts along dimension 0, may hold values from -6 to 6
- condition: bfloat16 [4096], P(('dp', 'sp')), parts along dimension 0, may hold values from -8 to 8
- context_latent: bfloat16 [1024, 256], P(('dp', 'sp')), parts along dimension 0, may hold values from -6 to 6
- context_rope: bfloat16 [1024, 64], P(('dp', 'sp')), parts along dimension 0, may hold values from -6 to 6
- shift_weight: bfloat16 [2048, 2048], P('sp', 'tp'), may hold values from -0.125 to 0.125
- scale_weight: bfloat16 [2048, 2048], P('sp', 'tp'), may hold values from -0.125 to 0.125
- gate_weight: bfloat16 [2048, 2048], P('sp', 'tp'), may hold values from -0.125 to 0.125
- norm_gain: float32 [2048], replicated, may hold values from 0.1 to 1.9
- down_query: bfloat16 [2048, 512], replicated, may hold values from -0.125 to 0.125
- down_latent: bfloat16 [2048, 256], replicated, may hold values from -0.125 to 0.125
- down_rope: bfloat16 [2048, 64], replicated, may hold values from -0.125 to 0.125
- query_gain: float32 [512], replicated, may hold values from 0.5 to 60
- latent_gain: float32 [256], replicated, may hold values from 0.1 to 1.9
- up_query: bfloat16 [512, 1536], P(None, 'tp'), may hold values from -0.25 to 0.25
- up_key: bfloat16 [256, 1024], P(None, 'tp'), may hold values from -0.375 to 0.375
- up_value: bfloat16 [256, 1024], P(None, 'tp'), may hold values from -0.375 to 0.375
- context_bias: float32 [8], P('tp'), may hold values from 1 to 2.5
- out_weight: bfloat16 [1024, 2048], replicated, may hold values from -3 to 3
Outputs:
- mixed_out: bfloat16 [3072, 2048], P(('dp', 'sp', 'tp')), parts along dimension 0
There are 2 independent parts, one for each index of `dp`. A program takes and returns all parts, laid end to end along the dimension named above; an argument that names none is the same for every part. Nothing has to cross between parts.
All inputs are finite; a program needn't handle non-finite values.
Results may differ from a plain program's by a relative error of at most 0.039.
The roundings to bfloat16 on the way count: a program that leaves them out, or rounds other values in their place, can miss the bound.
Values may be sent and summed in bfloat16 or wider, within the bound.
A program may use at most 128 MiB of HBM per device.

v0:
```python
import jax
import jax.numpy as jnp
from jax import lax
from jax.sharding import PartitionSpec as P

QK_NOPE = 128
QK_ROPE = 64
V_HEAD = 128
GRID_W = 64
epsilon = 1e-06
rope_base = 10000.0
block_limit = 2048


def rms_scaled(values, gain_vec):
    mean_sq = jnp.mean(values * values, axis=-1, keepdims=True)
    return values * lax.rsqrt(mean_sq + epsilon) * gain_vec


def rope_tables(positions, rope_width):
    freq_count = rope_width // 4
    inverse = rope_base ** (-jnp.arange(freq_count, dtype=jnp.float32) / freq_count)
    grid_row = (positions // GRID_W).astype(jnp.float32)
    grid_col = (positions % GRID_W).astype(jnp.float32)
    row_angle = grid_row[:, None] * inverse
    col_angle = grid_col[:, None] * inverse
    angles = jnp.concatenate([row_angle, row_angle, col_angle, col_angle], axis=-1)
    return (jnp.cos(angles), jnp.sin(angles))


def rope_turn(values, cosine_table, sine_table):
    part_one, part_two, part_three, part_four = jnp.split(values, 4, axis=-1)
    turned = jnp.concatenate([-part_two, part_one, -part_four, part_three], axis=-1)
    return values * cosine_table + turned * sine_table


def attend(attn_state, query_nope, query_rope, keys_nope, values_in, keys_rope, bias_col):
    score_scale = (query_nope.shape[-1] + query_rope.shape[-1]) ** (-0.5)
    scores = jnp.einsum("thd,khd->htk", query_nope, keys_nope, preferred_element_type=jnp.float32)
    scores = scores + jnp.einsum(
        "thr,kr->htk", query_rope, keys_rope, preferred_element_type=jnp.float32
    )
    scores = scores * score_scale + bias_col
    run_max, run_total, run_acc = attn_state
    new_max = jnp.maximum(run_max, jnp.max(scores, axis=-1))
    shrink = jnp.exp(run_max - new_max)
    weights = jnp.exp(scores - new_max[:, :, None])
    new_total = run_total * shrink + jnp.sum(weights, axis=-1)
    new_acc = run_acc * shrink[:, :, None] + jnp.einsum(
        "htk,khd->htd", weights.astype(jnp.bfloat16), values_in, preferred_element_type=jnp.float32
    )
    return (new_max, new_total, new_acc)


def over_blocks(attn_state, arrays, handle):
    row_count = arrays[0].shape[0]
    block_rows = 1
    for candidate in range(min(row_count, block_limit), 0, -1):
        if row_count % candidate == 0:
            block_rows = candidate
            break
    block_count = row_count // block_rows
    if block_count == 1:
        return handle(attn_state, arrays)
    stacked = tuple(
        (array_in.reshape((block_count, block_rows) + array_in.shape[1:]) for array_in in arrays)
    )

    def one_turn(inner_state, pieces):
        return (handle(inner_state, pieces), None)

    return lax.scan(one_turn, attn_state, stacked)[0]


def on_device(
    latent_in,
    condition,
    context_latent,
    context_rope,
    shift_weight,
    scale_weight,
    gate_weight,
    norm_gain,
    down_query,
    down_latent,
    down_rope,
    query_gain,
    latent_gain,
    up_query,
    up_key,
    up_value,
    context_bias,
    out_weight,
):
    activated = jax.nn.silu(condition.astype(jnp.float32)).astype(jnp.bfloat16)
    partials = jnp.stack(
        [
            jnp.dot(activated, weight_in, preferred_element_type=jnp.float32)
            for weight_in in (shift_weight, scale_weight, gate_weight)
        ]
    )
    summed = lax.psum(partials, "sp")
    modulation = lax.all_gather(summed, "tp", axis=1, tiled=True)
    shift_vec = modulation[0]
    scale_vec = modulation[1]
    gate_vec = modulation[2]
    residual_in = latent_in.astype(jnp.float32)
    normed = (rms_scaled(residual_in, norm_gain) * (1.0 + scale_vec) + shift_vec).astype(
        jnp.bfloat16
    )
    query_low = rms_scaled(
        jnp.dot(normed, down_query, preferred_element_type=jnp.float32), query_gain
    ).astype(jnp.bfloat16)
    latent_low = rms_scaled(
        jnp.dot(normed, down_latent, preferred_element_type=jnp.float32), latent_gain
    ).astype(jnp.bfloat16)
    local_rows = latent_in.shape[0]
    first_row = (lax.axis_index("sp") * lax.axis_size("tp") + lax.axis_index("tp")) * local_rows
    own_positions = first_row + jnp.arange(local_rows, dtype=jnp.int32)
    own_cosine, own_sine = rope_tables(own_positions, QK_ROPE)
    rope_keys = rope_turn(
        jnp.dot(normed, down_rope, preferred_element_type=jnp.float32), own_cosine, own_sine
    ).astype(jnp.bfloat16)
    query_group, latent_group, rope_group = (
        lax.all_gather(query_low, "tp", axis=0, tiled=True),
        lax.all_gather(latent_low, "tp", axis=0, tiled=True),
        lax.all_gather(rope_keys, "tp", axis=0, tiled=True),
    )
    group_rows = query_group.shape[0]
    group_positions = lax.axis_index("sp") * group_rows + jnp.arange(group_rows, dtype=jnp.int32)
    group_cosine, group_sine = rope_tables(group_positions, QK_ROPE)
    head_count = up_key.shape[1] // QK_NOPE
    queries = jnp.dot(query_group, up_query, preferred_element_type=jnp.float32).reshape(
        group_rows, head_count, QK_NOPE + QK_ROPE
    )
    query_nope = queries[:, :, :QK_NOPE].astype(jnp.bfloat16)
    query_rope = rope_turn(
        queries[:, :, QK_NOPE:], group_cosine[:, None, :], group_sine[:, None, :]
    ).astype(jnp.bfloat16)
    context_all, context_keys_rope = (
        lax.all_gather(context_latent, "sp", axis=0, tiled=True),
        lax.all_gather(context_rope, "sp", axis=0, tiled=True),
    )
    context_count = context_all.shape[0]
    context_nope = (
        jnp.dot(context_all, up_key, preferred_element_type=jnp.float32)
        .astype(jnp.bfloat16)
        .reshape(context_count, head_count, QK_NOPE)
    )
    context_values = (
        jnp.dot(context_all, up_value, preferred_element_type=jnp.float32)
        .astype(jnp.bfloat16)
        .reshape(context_count, head_count, V_HEAD)
    )
    start_state = (
        jnp.full((head_count, group_rows), -jnp.inf, jnp.float32),
        jnp.zeros((head_count, group_rows), jnp.float32),
        jnp.zeros((head_count, group_rows, V_HEAD), jnp.float32),
    )
    bias_col = context_bias[:, None, None]

    def context_step(inner_state, pieces):
        return attend(
            inner_state, query_nope, query_rope, pieces[0], pieces[1], pieces[2], bias_col
        )

    attn_state = over_blocks(
        start_state, (context_nope, context_values, context_keys_rope), context_step
    )
    own_nope = jnp.dot(latent_group, up_key, preferred_element_type=jnp.float32).astype(
        jnp.bfloat16
    )
    own_values = jnp.dot(latent_group, up_value, preferred_element_type=jnp.float32).astype(
        jnp.bfloat16
    )

    def expanded_step(inner_state, pieces):
        piece_rows = pieces[0].shape[0]
        return attend(
            inner_state,
            query_nope,
            query_rope,
            pieces[0].reshape(piece_rows, head_count, QK_NOPE),
            pieces[1].reshape(piece_rows, head_count, V_HEAD),
            pieces[2],
            0.0,
        )

    attn_state = over_blocks(
        attn_state,
        (
            lax.all_gather(own_nope, "sp", axis=0, tiled=True),
            lax.all_gather(own_values, "sp", axis=0, tiled=True),
            lax.all_gather(rope_group, "sp", axis=0, tiled=True),
        ),
        expanded_step,
    )
    attended = (attn_state[2] / attn_state[1][:, :, None]).astype(jnp.bfloat16)
    attended = attended.transpose(1, 0, 2).reshape(group_rows, head_count * V_HEAD)
    token_major = lax.all_to_all(attended, "tp", split_axis=0, concat_axis=1, tiled=True)
    mixed = jnp.dot(token_major, out_weight, preferred_element_type=jnp.float32)
    return (residual_in + gate_vec * mixed).astype(jnp.bfloat16)


def solution(mesh):
    in_specs = (
        P(("dp", "sp", "tp"), None),
        P(("dp", "sp")),
        P(("dp", "sp"), None),
        P(("dp", "sp"), None),
        P("sp", "tp"),
        P("sp", "tp"),
        P("sp", "tp"),
        P(),
        P(),
        P(),
        P(),
        P(),
        P(),
        P(None, "tp"),
        P(None, "tp"),
        P(None, "tp"),
        P("tp"),
        P(),
    )
    out_specs = P(("dp", "sp", "tp"), None)
    return jax.shard_map(
        on_device, mesh=mesh, in_specs=in_specs, out_specs=out_specs, check_vma=False
    )
```

profile of v0, /device:TPU:0, one launch (start us, length us, event | category | flops | bytes accessed | tf_op | source)
XLA Modules:
  0.0 158.6 jit_solution(2897633564219635338)
XLA Ops:
  1.3 1.2 fusion.72
  2.6 1.2 fusion.73
  3.8 1.3 fusion.74
  5.1 13.8 %psum.7 = f32[3,512]{1,0:T(4,128)S(1)} all-reduce(f32[3,512]{1,0:T(4,128)S(1)} %pad_maximum_fusion.2), channel_id=1, replica_groups=mesh['sp'=4,'tp'=4,'dp'=2] {'sp'}, use_global_device_ids=true, to_apply=%region_0.1 | all-reduce | flops 1536 | bytes 12288 | tf_op jit(solution)/shard_map/psum | solution.py:102
  18.9 8.2 %all_gather.27 = f32[3,2048]{1,0:T(4,128)S(1)} all-gather(f32[3,512]{1,0:T(4,128)S(1)} %psum.7), channel_id=1, replica_groups=mesh['sp'=4,'tp'=4,'dp'=2] {'tp'}, dimensions={1}, use_global_device_ids=true | all-gather | bytes 30720 | tf_op jit(solution)/shard_map/all_gather | solution.py:103
  27.1 1.2 fusion.26
  28.4 1.9 %multiply_reduce_fusion.1 = (f32[96]{0:T(128)S(1)}, f32[96,256]{1,0:T(8,128)S(1)}) fusion(bf16[2048,256]{1,0:T(8,128)(2,1)} %param.27, bf16[96,2048]{1,0:T(8,128)(2,1)} %param.18, f32[2048]{0:T(1024)S(1)} %bitcast.119, f32[2048]{0:T(1024)S(1)} %bitcast.122, f32[2048]{0:T(1024)} %param.25, f32[96]{0:T(128)S(1)} %add_rsqrt_fusion.2), kind=kOutput, calls=%fused_computation.50 | convolution fusion | flops 101892000 | bytes 1565440 | tf_op jit(solution)/shard_map/dot_general | solution.py:115
  30.3 8.7 %all_gather.31 = bf16[384,256]{1,0:T(8,128)(2,1)S(1)} all-gather(bf16[96,256]{1,0:T(8,128)(2,1)S(1)} %multiply_convert_fusion.1), channel_id=1, replica_groups=mesh['sp'=4,'tp'=4,'dp'=2] {'tp'}, dimensions={0}, use_global_device_ids=true | all-gather | bytes 245760 | tf_op jit(solution)/shard_map/all_gather | solution.py:126
  39.1 13.8 %all_gather.29 = bf16[512,256]{1,0:T(8,128)(2,1)S(1)} all-gather(bf16[128,256]{1,0:T(8,128)(2,1)S(1)} %copy-done.12), channel_id=1, replica_groups=mesh['sp'=4,'tp'=4,'dp'=2] {'sp'}, dimensions={0}, use_global_device_ids=true | all-gather | bytes 327680 | tf_op jit(solution)/shard_map/all_gather | solution.py:141
  52.9 0.9 convolution_convert_fusion.3
  54.0 1.0 convolution_convert_fusion
  56.0 8.5 %all_gather.28 = bf16[384,512]{1,0:T(8,128)(2,1)S(1)} all-gather(bf16[96,512]{1,0:T(8,128)(2,1)S(1)} %multiply_convert_fusion), channel_id=1, replica_groups=mesh['sp'=4,'tp'=4,'dp'=2] {'tp'}, dimensions={0}, use_global_device_ids=true | all-gather | bytes 491520 | tf_op jit(solution)/shard_map/all_gather | solution.py:125
  66.3 1.3 fusion.62
  69.6 0.9 fusion.47
  70.5 8.2 %all-gather = bf16[4,96,64]{1,2,0:T(8,128)(2,1)S(1)} all-gather(bf16[1,96,64]{1,2,0:T(8,128)(2,1)S(1)} %fusion.47), channel_id=1, replica_groups=mesh['sp'=4,'tp'=4,'dp'=2] {'tp'}, dimensions={0}, use_global_device_ids=true | all-gather | bytes 61440 | tf_op jit(solution)/shard_map/all_gather | solution.py:127
  79.4 1.6 reshape.254
  81.0 14.6 %all_gather.34 = bf16[1536,64]{0,1:T(8,128)(2,1)S(1)} all-gather(bf16[384,64]{0,1:T(8,128)(2,1)} %reshape.254), channel_id=1, replica_groups=mesh['sp'=4,'tp'=4,'dp'=2] {'sp'}, dimensions={0}, use_global_device_ids=true | all-gather | bytes 245760 | tf_op jit(solution)/shard_map/all_gather | solution.py:194
  95.6 16.9 %all_gather.32 = bf16[1536,256]{1,0:T(8,128)(2,1)S(1)} all-gather(bf16[384,256]{1,0:T(8,128)(2,1)} %convolution_convert_fusion.3), channel_id=1, replica_groups=mesh['sp'=4,'tp'=4,'dp'=2] {'sp'}, dimensions={0}, use_global_device_ids=true | all-gather | bytes 983040 | tf_op jit(solution)/shard_map/all_gather | solution.py:192
  112.9 12.2 %all_gather.30 = bf16[512,64]{0,1:T(8,128)(2,1)S(1)} all-gather(bf16[128,64]{0,1:T(8,128)(2,1)S(1)} %copy-done.13), channel_id=1, replica_groups=mesh['sp'=4,'tp'=4,'dp'=2] {'sp'}, dimensions={0}, use_global_device_ids=true | all-gather | bytes 81920 | tf_op jit(solution)/shard_map/all_gather | solution.py:142
  126.3 1.0 fusion.71
  128.3 15.6 %all_gather.35 = bf16[1536,256]{1,0:T(8,128)(2,1)S(1)} all-gather(bf16[384,256]{1,0:T(8,128)(2,1)S(1)} %convolution_convert_fusion.2), channel_id=1, replica_groups=mesh['sp'=4,'tp'=4,'dp'=2] {'sp'}, dimensions={0}, use_global_device_ids=true | all-gather | bytes 983040 | tf_op jit(solution)/shard_map/all_gather | solution.py:193
  145.5 0.9 fusion.23
  146.8 8.1 %all_to_all.19 = bf16[4,96,256]{2,1,0:T(8,128)(2,1)S(1)} all-to-all(bf16[4,96,256]{2,1,0:T(8,128)(2,1)S(1)} %all_to_all.14), channel_id=1, replica_groups=mesh['sp'=4,'tp'=4,'dp'=2] {'tp'}, dimensions={0} | all-to-all | bytes 393216 | tf_op jit(solution)/shard_map/all_to_all | solution.py:200
  154.9 3.8 %fusion.7 = bf16[96,2048]{1,0:T(8,128)(2,1)} fusion(bf16[96,1024]{1,0:T(8,128)(2,1)S(1)} %bitcast.116, bf16[1024,2048]{1,0:T(8,128)(2,1)} %param.35, bf16[96,2048]{1,0:T(8,128)(2,1)S(1)} %copy-done.1, f32[2048]{0:T(1024)S(1)} %bitcast.118), kind=kOutput, calls=%fused_computation.9 | convolution fusion | flops 403439616 | bytes 5185536 | tf_op jit(solution)/shard_map/dot_general | solution.py:201
  (80 shorter events, 11.5 us)
Async XLA Ops:
  0.0 55.3 %copy-start = (bf16[2048,512]{1,0:T(8,128)(2,1)S(1)}, bf16[2048,512]{1,0:T(8,128)(2,1)}, u32[]{:S(2)}) copy-start(bf16[2048,512]{1,0:T(8,128)(2,1)} %param.26) | copy-start | bytes 6291460
  0.0 30.2 %copy-start.19 = (f32[256]{0:T(256)S(1)}, f32[256]{0:T(256)}, u32[]{:S(2)}) copy-start(f32[256]{0:T(256)} %param.30) | copy-start | bytes 3076
  0.0 39.0 %copy-start.12 = (bf16[128,256]{1,0:T(8,128)(2,1)S(1)}, bf16[128,256]{1,0:T(8,128)(2,1)}, u32[]{:S(2)}) copy-start(bf16[128,256]{1,0:T(8,128)(2,1)} %param.20) | copy-start | bytes 196612
  1.3 51.5 %copy-start.3 = (bf16[256,256]{1,0:T(8,128)(2,1)S(1)}, bf16[256,256]{1,0:T(8,128)(2,1)}, u32[]{:S(2)}) copy-start(bf16[256,256]{1,0:T(8,128)(2,1)} %param.32) | copy-start | bytes 393220
  3.8 50.2 %copy-start.4 = (bf16[256,256]{1,0:T(8,128)(2,1)S(1)}, bf16[256,256]{1,0:T(8,128)(2,1)}, u32[]{:S(2)}) copy-start(bf16[256,256]{1,0:T(8,128)(2,1)} %param.33) | copy-start | bytes 393220
  27.1 28.1 %copy-start.14 = (f32[1,2048]{1,0:T(1,128)}, f32[1,2048]{1,0:T(1,128)S(1)}, u32[]{:S(2)}) copy-start(f32[1,2048]{1,0:T(1,128)S(1)} %get-tuple-element.15) | copy-start | bytes 24580
  27.1 27.9 %copy-start.5 = (bf16[256,256]{1,0:T(8,128)(2,1)S(1)}, bf16[256,256]{1,0:T(8,128)(2,1)}, u32[]{:S(2)}) copy-start(bf16[256,256]{1,0:T(8,128)(2,1)} %param.33) | copy-start | bytes 393220
  28.3 26.9 %copy-start.22 = (f32[96]{0:T(128)}, f32[96]{0:T(128)S(1)}, u32[]{:S(2)}) copy-start(f32[96]{0:T(128)S(1)} %add_rsqrt_fusion.2) | copy-start | bytes 1156
  28.3 26.9 %copy-start.1 = (bf16[96,2048]{1,0:T(8,128)(2,1)S(1)}, bf16[96,2048]{1,0:T(8,128)(2,1)}, u32[]{:S(2)}) copy-start(bf16[96,2048]{1,0:T(8,128)(2,1)} %param.18) | copy-start | bytes 1179652
  28.4 26.9 %copy-start.21 = (f32[2048]{0:T(1024)S(1)}, f32[2048]{0:T(1024)}, u32[]{:S(2)}) copy-start(f32[2048]{0:T(1024)} %param.25) | copy-start | bytes 24580
  53.7 2.2 %copy-start.17 = (f32[512]{0:T(512)S(1)}, f32[512]{0:T(512)}, u32[]{:S(2)}) copy-start(f32[512]{0:T(512)} %param.29) | copy-start | bytes 6148
  54.0 10.5 %copy-start.6 = (bf16[512,384]{1,0:T(8,128)(2,1)S(1)}, bf16[512,384]{1,0:T(8,128)(2,1)}, u32[]{:S(2)}) copy-start(bf16[512,384]{1,0:T(8,128)(2,1)} %param.31) | copy-start | bytes 1179652
  67.6 0.6 copy-start.11
  70.5 54.6 %copy-start.15 = (f32[384]{0:T(512)S(1)}, f32[384]{0:T(512)}, u32[]{:S(2)}) copy-start(f32[384]{0:T(512)} %get-tuple-element.33) | copy-start | bytes 4612
  70.5 54.6 %copy-start.16 = (f32[384]{0:T(512)S(1)}, f32[384]{0:T(512)}, u32[]{:S(2)}) copy-start(f32[384]{0:T(512)} %get-tuple-element.34) | copy-start | bytes 4612
  81.0 31.9 %copy-start.13 = (bf16[128,64]{0,1:T(8,128)(2,1)S(1)}, bf16[128,64]{0,1:T(8,128)(2,1)}, u32[]{:S(2)}) copy-start(bf16[128,64]{0,1:T(8,128)(2,1)} %param.21) | copy-start | bytes 49156
  81.0 44.1 %copy-start.18 = (f32[16]{0:T(128)S(1)}, f32[16]{0:T(128)}, u32[]{:S(2)}) copy-start(f32[16]{0:T(128)} %multiply_power_fusion) | copy-start | bytes 196
  81.0 44.4 %copy-start.7 = (f32[384,2,16]{0,2,1:T(8,128)S(1)}, f32[384,2,16]{0,2,1:T(8,128)}, u32[]{:S(2)}) copy-start(f32[384,2,16]{0,2,1:T(8,128)} %get-tuple-element.7) | copy-start | bytes 147460
  81.0 44.4 %copy-start.8 = (f32[384,2,16]{0,2,1:T(8,128)S(1)}, f32[384,2,16]{0,2,1:T(8,128)}, u32[]{:S(2)}) copy-start(f32[384,2,16]{0,2,1:T(8,128)} %get-tuple-element.8) | copy-start | bytes 147460
  81.0 44.4 %copy-start.9 = (f32[384,2,16]{0,2,1:T(8,128)S(1)}, f32[384,2,16]{0,2,1:T(8,128)}, u32[]{:S(2)}) copy-start(f32[384,2,16]{0,2,1:T(8,128)} %get-tuple-element.9) | copy-start | bytes 147460
  81.0 44.4 %copy-start.10 = (f32[384,2,16]{0,2,1:T(8,128)S(1)}, f32[384,2,16]{0,2,1:T(8,128)}, u32[]{:S(2)}) copy-start(f32[384,2,16]{0,2,1:T(8,128)} %get-tuple-element.10) | copy-start | bytes 147460
  126.3 1.0 copy-start.20
  143.8 1.0 copy-start.2
where the time goes:
time: 159 us
  blocking collectives  129 us (81%)
  matrix products  18.4 us (12%)
  other arithmetic  7.9 us (5%)
  local copies, waits for them, and re-layouts  3.43 us (2%)
    all_gather x1, blocking collectives, on_device(): lax.all_gather(own_nope, 'sp', axis=0, tiled=True)  16.9 us
    all_gather x1, blocking collectives, on_device(): lax.all_gather(own_values, 'sp', axis=0, tiled=True)  15.6 us
    all_gather x1, blocking collectives, on_device(): lax.all_gather(rope_group, 'sp', axis=0, tiled=True)  14.6 us
    all_gather x1, blocking collectives, on_device(): lax.all_gather(context_latent, 'sp', axis=0, tiled=True)  13.8 us
    psum x1, blocking collectives, on_device(): summed = lax.psum(partials, 'sp')  13.8 us
    all_gather x1, blocking collectives, on_device(): lax.all_gather(context_rope, 'sp', axis=0, tiled=True)  12.2 us
    all_gather x1, blocking collectives, on_device(): lax.all_gather(latent_low, 'tp', axis=0, tiled=True)  8.7 us
    all_gather x1, blocking collectives, on_device(): lax.all_gather(query_low, 'tp', axis=0, tiled=True)  8.53 us

commit v1 on v0

--- a/solution.py
+++ b/solution.py
@@ -100,7 +100,14 @@
         ]
     )
     summed = lax.psum(partials, "sp")
-    modulation = lax.all_gather(summed, "tp", axis=1, tiled=True)
+    n_dev = lax.axis_size("tp")
+    right = [(i, (i + 1) % n_dev) for i in range(n_dev)]
+    blocks = [summed]
+    for stride in range(1, n_dev):
+        blocks = [lax.ppermute(blocks[0], "tp", right), *blocks]
+    whole = jnp.concatenate(blocks, axis=1)
+    turn = (lax.axis_index("tp") + 1) * blocks[-1].shape[1]
+    modulation = jnp.roll(whole, turn, axis=1)
     shift_vec = modulation[0]
     scale_vec = modulation[1]
     gate_vec = modulation[2]

time: 159 us -> 153 us (0.962)
  blocking collectives: 129 us -> 123 us
  starting transfers between devices: 0 us -> 3.68 us
  local copies, waits for them, and re-layouts: 3.43 us -> 0.67 us
  other arithmetic: 7.9 us -> 5.41 us
  waiting for transfers between devices: 0 us -> 2.21 us
    all_gather x1 -> x0, blocking collectives: 8.2 us -> none  [on_device(): modulation = lax.all_gather(summed, 'tp', axis=1, tiled=True)]
    ppermute x0 -> x3, starting transfers between devices: none -> 3.68 us  [on_device(): blocks = [lax.ppermute(blocks[0], 'tp', right), *blocks]]
    ppermute x0 -> x3, waiting for transfers between devices: none -> 2.21 us  [on_device(): blocks = [lax.ppermute(blocks[0], 'tp', right), *blocks]]
    unnamed x47 -> x44, local copies, waits for them, and re-layouts: 2.39 us -> 0.25 us
  transfers between devices with their start and end apart: 0 -> 3, of which waited for: 0 -> 1; matrix products, arithmetic and copies ran while one was open for 0% -> 2% of each run, Pallas kernels for 0% -> 0%
where the time goes in v1:
time: 153 us; the launch traced here: 152 us
  blocking collectives  123 us (80%)
  matrix products  17.3 us (11%)
  other arithmetic  5.41 us (4%)
  starting transfers between devices  3.68 us (2%)
  waiting for transfers between devices  2.21 us (1%)
    all_gather x1, blocking collectives, on_device(): lax.all_gather(own_nope, 'sp', axis=0, tiled=True)  17.7 us
    all_gather x1, blocking collectives, on_device(): lax.all_gather(own_values, 'sp', axis=0, tiled=True)  15.6 us
    all_gather x1, blocking collectives, on_device(): lax.all_gather(rope_group, 'sp', axis=0, tiled=True)  14.1 us
    all_gather x1, blocking collectives, on_device(): lax.all_gather(context_latent, 'sp', axis=0, tiled=True)  14.1 us
    psum x1, blocking collectives, on_device(): summed = lax.psum(partials, 'sp')  13.7 us
    all_gather x1, blocking collectives, on_device(): lax.all_gather(context_rope, 'sp', axis=0, tiled=True)  12.6 us
    all_gather x1, blocking collectives, on_device(): lax.all_gather(query_low, 'tp', axis=0, tiled=True)  9.73 us
    all_gather x1, blocking collectives, on_device(): lax.all_gather(latent_low, 'tp', axis=0, tiled=True)  9.6 us
  transfers between devices with their start and end apart: 3, of which 1 were waited for; matrix products, arithmetic and copies ran while one was open for 2% of the time, Pallas kernels for 0%

profile of v1, /device:TPU:0, one launch (start us, length us, event | category | flops | bytes accessed | tf_op | source)
XLA Modules:
  0.0 152.2 jit_solution(15218846160885765642)
XLA Ops:
  0.9 1.3 fusion.71
  2.1 1.2 fusion.72
  3.4 1.2 fusion.73
  4.6 13.7 %psum.7 = f32[3,512]{1,0:T(4,128)S(1)} all-reduce(f32[3,512]{1,0:T(4,128)S(1)} %pad_maximum_fusion.2), channel_id=1, replica_groups=mesh['sp'=4,'tp'=4,'dp'=2] {'sp'}, use_global_device_ids=true, to_apply=%region_0.1 | all-reduce | flops 1536 | bytes 12288 | tf_op jit(solution)/shard_map/psum | solution.py:102
  18.4 1.5 %collective-permute-start = (f32[3,512]{1,0:T(4,128)S(1)}, f32[3,512]{1,0:T(4,128)S(1)}, u32[]{:S(2)}, u32[]{:S(2)}) collective-permute-start(f32[3,512]{1,0:T(4,128)S(1)} %psum.7), channel_id=1, source_target_pairs={{0,2},{2,4},{4,6},{6,0},{1,3},{3,5},{5,7},{7,1},{8,10},{10,12},{12... | collective-permute-start | bytes 18440 | tf_op jit(solution)/shard_map/ppermute | solution.py:107
  19.9 1.2 fusion.24
  21.1 14.1 %all_gather.25 = bf16[512,256]{1,0:T(8,128)(2,1)S(1)} all-gather(bf16[128,256]{1,0:T(8,128)(2,1)} %param.20), channel_id=1, replica_groups=mesh['sp'=4,'tp'=4,'dp'=2] {'sp'}, dimensions={0}, use_global_device_ids=true | all-gather | bytes 327680 | tf_op jit(solution)/shard_map/all_gather | solution.py:148
  36.6 1.5 %collective-permute-start.1 = (f32[3,512]{1,0:T(4,128)S(1)}, f32[3,512]{1,0:T(4,128)S(1)}, u32[]{:S(2)}, u32[]{:S(2)}) collective-permute-start(f32[3,512]{1,0:T(4,128)S(1)} %collective-permute-done), channel_id=1, source_target_pairs={{0,2},{2,4},{4,6},{6,0},{1,3},{3,5},{5,7},{7,1},{8,10},{10,12},{12... | collective-permute-start | bytes 18440 | tf_op jit(solution)/shard_map/ppermute | solution.py:107
  38.1 0.9 fusion.41
  39.0 2.2 %collective-permute-done.1 = f32[3,512]{1,0:T(4,128)S(1)} collective-permute-done((f32[3,512]{1,0:T(4,128)S(1)}, f32[3,512]{1,0:T(4,128)S(1)}, u32[]{:S(2)}, u32[]{:S(2)}) %collective-permute-start.1) | collective-permute-done | bytes 6176 | tf_op jit(solution)/shard_map/ppermute | solution.py:107
  41.8 12.6 %all_gather.26 = bf16[512,64]{0,1:T(8,128)(2,1)} all-gather(bf16[128,64]{0,1:T(8,128)(2,1)S(1)} %copy-done.9), channel_id=1, replica_groups=mesh['sp'=4,'tp'=4,'dp'=2] {'sp'}, dimensions={0}, use_global_device_ids=true | all-gather | bytes 81920 | tf_op jit(solution)/shard_map/all_gather | solution.py:149
  54.7 1.7 %multiply_reduce_fusion.1 = (f32[96]{0:T(128)S(1)}, f32[96,256]{1,0:T(8,128)S(1)}) fusion(bf16[2048,256]{1,0:T(8,128)(2,1)} %param.27, bf16[96,2048]{1,0:T(8,128)(2,1)S(1)} %copy-done.1, f32[2048]{0:T(1024)S(1)} %bitcast.122, f32[2048]{0:T(1024)S(1)} %bitcast.119, f32[2048]{0:T(1024)S(1)} %copy-done.16, f32[96]{0:T(128)S(1)} %add_rsqrt_fusion.2), kind=kOutput, calls=%fused_computation.49 | convolution fusion | flops 101892000 | bytes 1565440 | tf_op jit(solution)/shard_map/dot_general | solution.py:122
  56.5 9.6 %all_gather.27 = bf16[384,256]{1,0:T(8,128)(2,1)S(1)} all-gather(bf16[96,256]{1,0:T(8,128)(2,1)S(1)} %multiply_convert_fusion.1), channel_id=1, replica_groups=mesh['sp'=4,'tp'=4,'dp'=2] {'tp'}, dimensions={0}, use_global_device_ids=true | all-gather | bytes 245760 | tf_op jit(solution)/shard_map/all_gather | solution.py:133
  66.5 1.1 fusion.61
  67.7 7.2 %all-gather = bf16[4,96,64]{1,2,0:T(8,128)(2,1)S(1)} all-gather(bf16[1,96,64]{1,2,0:T(8,128)(2,1)S(1)} %fusion.46), channel_id=1, replica_groups=mesh['sp'=4,'tp'=4,'dp'=2] {'tp'}, dimensions={0}, use_global_device_ids=true | all-gather | bytes 61440 | tf_op jit(solution)/shard_map/all_gather | solution.py:134
  75.1 14.1 %all_gather.30 = bf16[1536,64]{0,1:T(8,128)(2,1)S(1)} all-gather(bf16[384,64]{0,1:T(8,128)(2,1)S(1)} %reshape.254), channel_id=1, replica_groups=mesh['sp'=4,'tp'=4,'dp'=2] {'sp'}, dimensions={0}, use_global_device_ids=true | all-gather | bytes 245760 | tf_op jit(solution)/shard_map/all_gather | solution.py:201
  89.3 1.4 multiply_reduce_fusion
  90.8 9.7 %all_gather.24 = bf16[384,512]{1,0:T(8,128)(2,1)S(1)} all-gather(bf16[96,512]{1,0:T(8,128)(2,1)S(1)} %multiply_convert_fusion), channel_id=1, replica_groups=mesh['sp'=4,'tp'=4,'dp'=2] {'tp'}, dimensions={0}, use_global_device_ids=true | all-gather | bytes 491520 | tf_op jit(solution)/shard_map/all_gather | solution.py:132
  101.0 17.7 %all_gather.28 = bf16[1536,256]{1,0:T(8,128)(2,1)S(1)} all-gather(bf16[384,256]{1,0:T(8,128)(2,1)S(1)} %convolution_convert_fusion.3), channel_id=1, replica_groups=mesh['sp'=4,'tp'=4,'dp'=2] {'sp'}, dimensions={0}, use_global_device_ids=true | all-gather | bytes 983040 | tf_op jit(solution)/shard_map/all_gather | solution.py:199
  120.0 1.0 fusion.70
  121.9 15.6 %all_gather.31 = bf16[1536,256]{1,0:T(8,128)(2,1)S(1)} all-gather(bf16[384,256]{1,0:T(8,128)(2,1)S(1)} %convolution_convert_fusion.2), channel_id=1, replica_groups=mesh['sp'=4,'tp'=4,'dp'=2] {'sp'}, dimensions={0}, use_global_device_ids=true | all-gather | bytes 983040 | tf_op jit(solution)/shard_map/all_gather | solution.py:200
  139.1 0.9 fusion.21
  140.3 8.1 %all_to_all.19 = bf16[4,96,256]{2,1,0:T(8,128)(2,1)S(1)} all-to-all(bf16[4,96,256]{2,1,0:T(8,128)(2,1)S(1)} %all_to_all.14), channel_id=1, replica_groups=mesh['sp'=4,'tp'=4,'dp'=2] {'tp'}, dimensions={0} | all-to-all | bytes 393216 | tf_op jit(solution)/shard_map/all_to_all | solution.py:207
  148.4 3.8 %fusion.29 = bf16[96,2048]{1,0:T(8,128)(2,1)} fusion(bf16[96,2048]{1,0:T(8,128)(2,1)S(1)} %copy-done.1, f32[2048]{0:T(1024)S(1)} %bitcast.118, bf16[96,1024]{1,0:T(8,128)(2,1)S(1)} %bitcast.116, bf16[1024,2048]{1,0:T(8,128)(2,1)} %param.35), kind=kOutput, calls=%fused_computation.32 | convolution fusion | flops 403439616 | bytes 5185536 | tf_op jit(solution)/shard_map/dot_general | solution.py:208
  (83 shorter events, 8.4 us)
Async XLA Ops:
  0.0 89.3 %copy-start = (bf16[2048,512]{1,0:T(8,128)(2,1)S(1)}, bf16[2048,512]{1,0:T(8,128)(2,1)}, u32[]{:S(2)}) copy-start(bf16[2048,512]{1,0:T(8,128)(2,1)} %param.26) | copy-start | bytes 6291460
  0.0 54.6 %copy-start.1 = (bf16[96,2048]{1,0:T(8,128)(2,1)S(1)}, bf16[96,2048]{1,0:T(8,128)(2,1)}, u32[]{:S(2)}) copy-start(bf16[96,2048]{1,0:T(8,128)(2,1)} %param.18) | copy-start | bytes 1179652
  0.0 35.3 %copy-start.2 = (bf16[256,256]{1,0:T(8,128)(2,1)S(1)}, bf16[256,256]{1,0:T(8,128)(2,1)}, u32[]{:S(2)}) copy-start(bf16[256,256]{1,0:T(8,128)(2,1)} %param.32) | copy-start | bytes 393220
  0.0 35.5 %copy-start.3 = (bf16[256,256]{1,0:T(8,128)(2,1)S(1)}, bf16[256,256]{1,0:T(8,128)(2,1)}, u32[]{:S(2)}) copy-start(bf16[256,256]{1,0:T(8,128)(2,1)} %param.33) | copy-start | bytes 393220
  0.0 41.8 %copy-start.9 = (bf16[128,64]{0,1:T(8,128)(2,1)S(1)}, bf16[128,64]{0,1:T(8,128)(2,1)}, u32[]{:S(2)}) copy-start(bf16[128,64]{0,1:T(8,128)(2,1)} %param.21) | copy-start | bytes 49156
  0.0 54.6 %copy-start.16 = (f32[2048]{0:T(1024)S(1)}, f32[2048]{0:T(1024)}, u32[]{:S(2)}) copy-start(f32[2048]{0:T(1024)} %param.25) | copy-start | bytes 24580
  4.6 51.8 %copy-start.13 = (f32[256]{0:T(256)S(1)}, f32[256]{0:T(256)}, u32[]{:S(2)}) copy-start(f32[256]{0:T(256)} %param.30) | copy-start | bytes 3076
  18.4 18.2 %collective-permute-start = (f32[3,512]{1,0:T(4,128)S(1)}, f32[3,512]{1,0:T(4,128)S(1)}, u32[]{:S(2)}, u32[]{:S(2)}) collective-permute-start(f32[3,512]{1,0:T(4,128)S(1)} %psum.7), channel_id=1, source_target_pairs={{0,2},{2,4},{4,6},{6,0},{1,3},{3,5},{5,7},{7,1},{8,10},{10,12},{12... | collective-permute-start | bytes 18440 | tf_op jit(solution)/shard_map/ppermute | solution.py:107
  36.6 19.9 %copy-start.17 = (f32[96]{0:T(128)}, f32[96]{0:T(128)S(1)}, u32[]{:S(2)}) copy-start(f32[96]{0:T(128)S(1)} %add_rsqrt_fusion.2) | copy-start | bytes 1156
  36.6 4.6 %collective-permute-start.1 = (f32[3,512]{1,0:T(4,128)S(1)}, f32[3,512]{1,0:T(4,128)S(1)}, u32[]{:S(2)}, u32[]{:S(2)}) collective-permute-start(f32[3,512]{1,0:T(4,128)S(1)} %collective-permute-done), channel_id=1, source_target_pairs={{0,2},{2,4},{4,6},{6,0},{1,3},{3,5},{5,7},{7,1},{8,10},{10,12},{12... | collective-permute-start | bytes 18440 | tf_op jit(solution)/shard_map/ppermute | solution.py:107
  41.2 13.2 %collective-permute-start.2 = (f32[3,512]{1,0:T(4,128)S(1)}, f32[3,512]{1,0:T(4,128)S(1)}, u32[]{:S(2)}, u32[]{:S(2)}) collective-permute-start(f32[3,512]{1,0:T(4,128)S(1)} %collective-permute-done.1), channel_id=1, source_target_pairs={{0,2},{2,4},{4,6},{6,0},{1,3},{3,5},{5,7},{7,1},{8,10},{10,12},{12... | collective-permute-start | bytes 18440 | tf_op jit(solution)/shard_map/ppermute | solution.py:107
  54.4 12.1 %copy-start.15 = (bf16[2048,64]{0,1:T(8,128)(2,1)S(1)}, bf16[2048,64]{0,1:T(8,128)(2,1)}, u32[]{:S(2)}) copy-start(bf16[2048,64]{0,1:T(8,128)(2,1)} %param.28) | copy-start | bytes 786436
  54.6 20.3 %copy-start.10 = (f32[1,2048]{1,0:T(1,128)}, f32[1,2048]{1,0:T(1,128)S(1)}, u32[]{:S(2)}) copy-start(f32[1,2048]{1,0:T(1,128)S(1)} %get-tuple-element.12) | copy-start | bytes 24580
  54.6 20.3 %copy-start.11 = (f32[1,2048]{1,0:T(1,128)}, f32[1,2048]{1,0:T(1,128)S(1)}, u32[]{:S(2)}) copy-start(f32[1,2048]{1,0:T(1,128)S(1)} %get-tuple-element.13) | copy-start | bytes 24580
  54.7 12.9 %copy-start.8 = (f32[96,16]{0,1:T(8,128)S(1)}, f32[96,16]{0,1:T(8,128)}, u32[]{:S(2)}) copy-start(f32[96,16]{0,1:T(8,128)} %get-tuple-element.22) | copy-start | bytes 18436
  66.5 24.1 %copy-start.12 = (f32[512]{0:T(512)S(1)}, f32[512]{0:T(512)}, u32[]{:S(2)}) copy-start(f32[512]{0:T(512)} %param.29) | copy-start | bytes 6148
  75.1 25.4 %copy-start.4 = (bf16[512,384]{1,0:T(8,128)(2,1)S(1)}, bf16[512,384]{1,0:T(8,128)(2,1)}, u32[]{:S(2)}) copy-start(bf16[512,384]{1,0:T(8,128)(2,1)} %param.31) | copy-start | bytes 1179652
  100.5 18.6 %copy-start.5 = (f32[384,64]{0,1:T(8,128)S(1)}, f32[384,64]{0,1:T(8,128)}, u32[]{:S(2)}) copy-start(f32[384,64]{0,1:T(8,128)} %get-tuple-element.14) | copy-start | bytes 294916
  100.5 18.6 %copy-start.6 = (f32[384,64]{0,1:T(8,128)S(1)}, f32[384,64]{0,1:T(8,128)}, u32[]{:S(2)}) copy-start(f32[384,64]{0,1:T(8,128)} %get-tuple-element.15) | copy-start | bytes 294916
  119.9 1.0 copy-start.7
  120.0 1.0 copy-start.14
